TPU v7x, 32 devices: a whole 2x2x4 slice. The times are simulated.
32 devices in a mesh: sp: 8 (over z, y), tp: 4 (over x, core).
Axes of the slice: x: 2, y: 2, z: 4, core: 2. Of those that a mesh axis runs over, the one named last changes fastest.
Arguments:
- query_first: bfloat16 [6144, 8, 128], P('sp', 'tp'), may hold values from -5.375 to 5.375
- key_first: bfloat16 [6144, 8, 128], P('sp', 'tp'), may hold values from -5.375 to 5.375
- value_first: bfloat16 [6144, 8, 128], P('sp', 'tp'), may hold values from -6 to 6
- query_second: bfloat16 [6144, 8, 256], P('sp', 'tp'), may hold values from -5.375 to 5.375
- key_second: bfloat16 [6144, 8, 256], P('sp', 'tp'), may hold values from -5.375 to 5.375
- value_second: bfloat16 [6144, 8, 128], P('sp', 'tp'), may hold values from -6 to 6
- mix_lambda: float32 [2, 8], P(None, 'tp'), may hold values from 0.3 to 0.8
- head_gain: float32 [2, 8, 128], P(None, 'tp'), may hold values from 0.1 to 1.9
- out_weight: bfloat16 [2, 8, 128, 2048], P(None, 'tp'), may hold values from -0.125 to 0.125
- residual: bfloat16 [6144, 2048], P(('sp', 'tp')), may hold values from -6 to 6
- norm_gain: float32 [2, 2048], replicated, may hold values from 0.1 to 1.9
- up_weight: bfloat16 [2048, 8192], P('sp', 'tp'), may hold values from -0.125 to 0.125
- down_weight: bfloat16 [8192, 2048], P('tp', 'sp'), may hold values from -0.0625 to 0.0625
Outputs:
- mixed: bfloat16 [6144, 2048], P(('sp', 'tp'))
All inputs are finite; a program needn't handle non-finite values.
Results may differ from a plain program's by a relative error of at most 0.02.
Values may be sent and summed in bfloat16 or wider, within the bound.
A program may use at most 128 MiB of HBM per device.

v0:
```python
import functools
import math

import jax
import jax.numpy as jnp
from jax import lax
from jax.experimental import pallas as pl
from jax.experimental.pallas import tpu as pltpu
from jax.sharding import PartitionSpec as P

MESH = pl.DeviceIdType.MESH
EPSILON = 1e-05
BF16 = jnp.bfloat16
F32 = jnp.float32
GROUP = 2
UP, DOWN = 0, 1
Q1, Q2, K1, K2, V1 = range(5)


def when(condition):
    return pl.when(condition)


def branches(index, count, body):
    for k in range(count):
        pl.when(index == k)(functools.partial(body, k))


def xor(left, bits):
    result, weight = 0, 1
    while bits:
        low = lax.rem(lax.div(left, weight), 2)
        result = result + weight * (1 - low if bits % 2 else low)
        bits, weight = bits // 2, weight * 2
    return result + left - lax.rem(left, weight)


def aligned(value, unit):
    return pl.multiple_of(value, unit)


def layer_norm(rows, scales):
    average = jnp.mean(rows, axis=-1, keepdims=True)
    centred = rows - average
    spread = jnp.mean(centred * centred, axis=-1, keepdims=True)
    return centred * lax.rsqrt(spread + EPSILON) * scales


def combo_order(heads):
    order = []
    for h in range(heads):
        order += [(0, h), (1, h)] if h % 2 == 0 else [(1, h), (0, h)]
    return order


class Sizes:
    def __init__(self, n_sp, n_tp, heads, tokens, value, width, sub, hidden):
        self.n_sp, self.n_tp, self.heads = n_sp, n_tp, heads
        self.combos = combo_order(heads)
        self.A = len(self.combos)
        self.B = n_sp // self.A
        self.F = n_sp // GROUP
        self.tokens, self.value = tokens, value
        self.rows = tokens // n_tp
        self.width, self.sub = width, sub
        self.hidden = hidden // GROUP
        self.chips = GROUP * n_tp // 2
        self.order = range(self.A - 1, 0, -1)


def slots(kind):
    return (Q1, K1, V1) if kind == 0 else (Q1, Q2, K1, K2, V1)


def body(
    z,
    scales,
    query_block,
    key_block,
    lam_ref,
    gain_ref,
    norm_ref,
    residual_ref,
    qf,
    kf,
    vf,
    qs,
    ks,
    vs,
    ow_in,
    up_in,
    down_in,
    out_ref,
    qb,
    kb,
    vw,
    head_out,
    gathered,
    ow,
    wup,
    wdn,
    x_all,
    normed_ref,
    own_part,
    s1_out,
    s1_in,
    s2_out,
    s2_in,
    qkv_send,
    qkv_recv,
    kv_send,
    kv_recv,
    local_sem,
    swap_send,
    swap_recv,
    wz_send,
    wz_recv,
    wlocal_sem,
    ow_send,
    ow_recv,
    owlocal_sem,
    o_send,
    o_recv,
    x_send,
    xf_send,
    x_recv,
    s1_send,
    s1_recv,
    s2_send,
    s2_recv,
):
    s, t = lax.axis_index("sp"), lax.axis_index("tp")
    A, B, F, n_sp, n_tp = z.A, z.B, z.F, z.n_sp, z.n_tp
    a, b = lax.div(s, B), lax.rem(s, B)
    f, g = lax.div(s, GROUP), lax.rem(s, GROUP)
    chip, core = g * (n_tp // 2) + lax.div(t, 2), lax.rem(t, 2)
    pair = (s, t + 1 - 2 * core)
    TD, VD, R, sub, hidden = z.tokens, z.value, z.rows, z.sub, z.hidden
    half = qb.shape[2]

    def remote(src, dst, send, recv, device):
        return pltpu.make_async_remote_copy(
            src_ref=src, dst_ref=dst, send_sem=send, recv_sem=recv, device_id=device, device_id_type=MESH
        )

    vw[:, VD:] = jnp.ones((vw.shape[0], VD), BF16)
    barrier = pltpu.get_barrier_semaphore()
    for i in range(n_sp):
        for j in range(n_tp):
            @when((s != i) | (t != j))
            def greet():
                pl.semaphore_signal(barrier, inc=1, device_id=(i, j), device_id_type=MESH)
    pl.semaphore_wait(barrier, n_sp * n_tp - 1)

    def source(i, slot):
        kind, h = z.combos[i]
        if kind == 0:
            return {Q1: qf, K1: kf, V1: vf}[slot].at[h]
        if slot == V1:
            return vs.at[h]
        return (qs if slot < K1 else ks).at[h, slot % 2]

    def target(slot, origin, member):
        if slot < K1:
            return qb.at[slot, pl.ds(aligned(origin * TD, TD), TD), :]
        row = pl.ds(aligned((origin * B + member) * TD, TD), TD)
        if slot < V1:
            return kb.at[slot - K1, row, :]
        return vw.at[row, pl.ds(0, VD)]

    def qkv(me, i, slot):
        return remote(
            source(i, slot), target(slot, me, b), qkv_send.at[i, slot], qkv_recv.at[me, slot], (i * B + b, t)
        )

    def qkv_arrival(origin, slot):
        place = target(slot, origin, b)
        return remote(place, place, qkv_send.at[0, slot], qkv_recv.at[origin, slot], (s, t))

    def qkv_local(me, slot):
        return pltpu.make_async_copy(source(me, slot), target(slot, me, b), local_sem.at[slot])

    def kv(me, origin, other, slot):
        src = source(me, slot) if origin == me else target(slot, origin, b)
        return remote(
            src, target(slot, origin, b), kv_send.at[origin, other, slot - K1], kv_recv.at[origin, b, slot - K1],
            (me * B + other, t),
        )

    def kv_arrival(origin, member, slot):
        place = target(slot, origin, member)
        return remote(place, place, kv_send.at[0, 0, 0], kv_recv.at[origin, member, slot - K1], (s, t))

    def peers(count, mine, action):
        for k in range(count):
            pl.when(mine != k)(functools.partial(action, k))

    def near(me):
        return sorted((i for i in range(A) if i != me), key=lambda i: abs(i - me))

    @functools.partial(branches, a, A)
    def send_heads(me):
        for i in reversed(near(me)):
            for slot in reversed(slots(z.combos[i][0])):
                qkv(me, i, slot).start()
        mine = slots(z.combos[me][0])
        for slot in mine:
            qkv_local(me, slot).start()

        def share(other):
            for slot in mine:
                if slot >= K1:
                    kv(me, me, other, slot).start()

        peers(B, b, share)

    def wplace(kind, block):
        if kind == UP:
            return wup.at[pl.ds(aligned(block * sub, sub), sub), :]
        return wdn.at[block]

    def wsource(kind, half):
        window = pl.ds(aligned(half * hidden, hidden), hidden)
        return up_in.at[:, window] if kind == UP else down_in.at[window, :]

    def swap(kind):
        return remote(
            wsource(kind, 1 - g), wplace(kind, s), swap_send.at[kind], swap_recv.at[kind], (f * GROUP + 1 - g, t)
        )

    def swap_arrival(kind):
        place = wplace(kind, f * GROUP + 1 - g)
        return remote(place, place, swap_send.at[kind], swap_recv.at[kind], (s, t))

    def wlocal(kind):
        return pltpu.make_async_copy(wsource(kind, g), wplace(kind, s), wlocal_sem.at[kind])

    def along(me, origin, index, kind, direction, raw=False):
        j = g if index == 0 else 1 - g
        place = wplace(kind, origin * GROUP + j)
        src = wsource(kind, g) if raw else place
        return remote(
            src, place, wz_send.at[(direction + 1) // 2, origin, index, kind], wz_recv.at[origin, index, kind],
            ((me + direction) * GROUP + g, t),
        )

    def relay(events):
        if not events:
            return

        @functools.partial(branches, f, F)
        def pass_on(me):
            for k, index, kind in events:
                for direction in (1, -1):
                    origin = me - direction * k
                    if 0 <= origin < F:
                        move = along(me, origin, index, kind, direction)
                        move.wait_recv()
                        if 0 <= me + direction < F:
                            move.start()

    events = [(k, index, kind) for k in range(1, F) for index in range(2) for kind in (UP, DOWN)]

    for kind in (UP, DOWN):
        swap(kind).start()
        wlocal(kind).start()

    @functools.partial(branches, f, F)
    def send_own(me):
        for kind in (UP, DOWN):
            for direction in (1, -1):
                if 0 <= me + direction < F:
                    along(me, me, 0, kind, direction, raw=True).start()

    def ow_rows(i):
        kind, h = z.combos[i]
        return ow_in.at[pl.ds((kind * z.heads + h) * VD, VD), :]

    def ow_place(owner, i):
        return ow.at[pl.ds(aligned((owner * A + i) * VD, VD), VD), :]

    def ow_copy(i, other):
        return remote(ow_rows(i), ow_place(t, i), ow_send.at[other, i], ow_recv.at[t, i], (s, other))

    def ow_local(i):
        return pltpu.make_async_copy(ow_rows(i), ow_place(t, i), owlocal_sem.at[i])

    def ow_arrival(owner, i):
        place = ow_place(owner, i)
        return remote(place, place, ow_send.at[0, 0], ow_recv.at[owner, i], (s, t))

    for i in range(A):
        ow_local(i).start()
    peers(n_tp, t, lambda other: [ow_copy(i, other).start() for i in range(A)] and None)

    @functools.partial(branches, a, A)
    def receive_heads(me):
        mine = slots(z.combos[me][0])
        for origin in near(me):
            for slot in mine:
                if slot >= K1:
                    qkv_arrival(origin, slot).wait_recv()

            def share(other):
                for slot in mine:
                    if slot >= K1:
                        kv(me, origin, other, slot).start()

            peers(B, b, share)

    for kind in (UP, DOWN):
        swap_arrival(kind).wait_recv()

    @functools.partial(branches, f, F)
    def send_swapped(me):
        for kind in (UP, DOWN):
            for direction in (1, -1):
                if 0 <= me + direction < F:
                    along(me, me, 1, kind, direction).start()

    @functools.partial(branches, a, A)
    def receive_rest(me):
        mine = slots(z.combos[me][0])
        for slot in mine:
            qkv_local(me, slot).wait()
            if slot < K1:
                for origin in near(me):
                    qkv_arrival(origin, slot).wait_recv()
            else:
                for origin in range(A):
                    peers(B, b, lambda other: kv_arrival(origin, other, slot).wait_recv())

    second = sum(jnp.where(a == i, kind, 0) for i, (kind, h) in enumerate(z.combos))

    @when(second == 0)
    def split_maps():
        low = lax.broadcasted_iota(jnp.int32, (TD, half), 1) < half // 2
        for block in range(A):
            rows = pl.ds(block * TD, TD)
            queries = qb[0, rows, :]
            empty = jnp.zeros_like(queries)
            qb[1, rows, :] = jnp.where(low, empty, queries)
            qb[0, rows, :] = jnp.where(low, queries, empty)

    factor = jnp.where(second == 0, scales[0], scales[1]) * math.log2(math.e)
    lam = lam_ref[a]
    gain = gain_ref[pl.ds(a, 1), :]

    def attend(row):
        maxima, sums = [None, None], [None, None]
        window = pl.ds(aligned(row, query_block), query_block)
        for start in range(0, n_sp * TD, key_block):
            for c in range(2):
                scores = lax.dot_general(
                    qb[c, window, :],
                    kb[second * c, start : start + key_block, :],
                    (((1,), (1,)), ((), ())),
                    preferred_element_type=F32,
                )
                newest = jnp.max(scores, axis=-1, keepdims=True)
                if start:
                    newest = jnp.maximum(maxima[c], newest)
                weights = jnp.exp2((scores - newest) * factor).astype(BF16)
                summed = jnp.dot(weights, vw[start : start + key_block, :], preferred_element_type=F32)
                if start:
                    summed = summed + sums[c] * jnp.exp2((maxima[c] - newest) * factor)
                maxima[c], sums[c] = newest, summed
        one, two = (member[:, :VD] / member[:, VD:] for member in sums)
        attended = one - lam * two
        mean_square = jnp.mean(attended * attended, axis=-1, keepdims=True)
        head_out[window, :] = (attended * lax.rsqrt(mean_square + EPSILON) * gain).astype(BF16)

    def outs(n, owner, other):
        rows = pl.ds(aligned(owner * TD + other * R, R), R)
        return remote(
            head_out.at[rows, :], gathered.at[t * A + a], o_send.at[n, other], o_recv.at[t * A + a],
            (owner * B + b, other),
        )

    def outs_arrival(index):
        place = gathered.at[index]
        return remote(place, place, o_send.at[0, 0], o_recv.at[index], (s, t))

    early = {0: events[0:2], 1: events[2:3], 2: events[3:4], 3: events[4:6]}

    def attention_step(n, carry):
        owner = lax.rem(a + 1 + n, A)

        def inner(m, unused):
            attend(owner * TD + m * query_block)
            return unused

        lax.fori_loop(0, TD // query_block, inner, 0)
        for other in range(n_tp):
            @when((n < A - 1) | (t != other))
            def send():
                outs(n, owner, other).start()
        for point in range(min(A, len(early))):
            pl.when(n == point)(functools.partial(relay, early[point]))
        return carry

    lax.fori_loop(0, A, attention_step, 0)
    gathered[t * A + a] = head_out[pl.ds(aligned(a * TD + t * R, R), R), :]
    used = sum(len(early[point]) for point in range(min(A, len(early))))

    for i in range(A):
        ow_local(i).wait()
    for owner in range(n_tp):
        @when(t != owner)
        def weights_arrive():
            for i in range(A):
                ow_arrival(owner, i).wait_recv()
    for index in range(n_tp * A):
        pl.when((t != index // A) | (a != index % A))(lambda: outs_arrival(index).wait_recv())

    left = jnp.concatenate([gathered[index] for index in range(n_tp * A)], axis=1)
    projected = jnp.dot(left, ow[...], preferred_element_type=F32) + residual_ref[...].astype(F32)
    normed = layer_norm(projected, norm_ref[0:1, :])
    normed_ref[...] = normed
    x_all[chip * 2 + core] = normed.astype(BF16)

    def chip_at(n):
        return xor(chip, n)

    def device_of(index, c):
        return (f * GROUP + lax.div(index, n_tp // 2), lax.rem(index, n_tp // 2) * 2 + c)

    def rows_to_chip(n):
        place = x_all.at[chip * 2 + core]
        return remote(place, place, x_send.at[n], x_recv.at[chip * 2 + core], device_of(chip_at(n), core))

    def rows_to_pair(n):
        index = chip_at(n) * 2 + core
        return remote(x_all.at[index], x_all.at[index], xf_send.at[n], x_recv.at[index], pair)

    def rows_arrival(index):
        place = x_all.at[index]
        return remote(place, place, x_send.at[0], x_recv.at[index], (s, t))

    rows_to_pair(0).start()
    for n in range(z.chips - 1, 0, -1):
        rows_to_chip(n).start()

    relay(events[used:])
    for kind in (UP, DOWN):
        wlocal(kind).wait()

    def half_to_pair(n):
        return remote(s1_out.at[n], s1_in.at[n], s1_send.at[n], s1_recv.at[n], pair)

    def sum_to_chip(n):
        return remote(s2_out.at[n], s2_in.at[n], s2_send.at[n], s2_recv.at[n], device_of(chip_at(n), core))

    def feed(n):
        index = chip_at(n)
        if n:
            rows_arrival(index * 2 + core).wait_recv()
            rows_to_pair(n).start()
        rows_arrival(index * 2 + 1 - core).wait_recv()
        for c in range(2):
            expanded = jnp.dot(x_all[index * 2 + c], wup[...], preferred_element_type=F32)
            acted = jnp.square(jnp.maximum(expanded, 0.0)).astype(BF16)

            def columns(block, unused):
                part = jnp.dot(acted, wdn[block], preferred_element_type=F32)
                window = pl.ds(aligned(block * sub, sub), sub)

                @when(core == c)
                def keep():
                    own_part[n, :, window] = part

                @when(core != c)
                def give():
                    s1_out[n, :, window] = part.astype(BF16)

                return unused

            for block in range(n_sp):
                columns(block, 0)
        half_to_pair(n).start()

    def reduce(n):
        half_to_pair(n).wait_recv()
        s2_out[n] = (own_part[n] + s1_in[n].astype(F32)).astype(BF16)
        sum_to_chip(n).start()

    for n in range(z.chips):
        feed(n)
        if n > 1:
            reduce(n - 1)
    reduce(z.chips - 1)

    half_to_pair(0).wait_recv()
    total = normed_ref[...] + own_part[0] + s1_in[0].astype(F32)
    for n in range(1, z.chips):
        sum_to_chip(n).wait_recv()
        total = total + s2_in[n].astype(F32)
    out_ref[...] = layer_norm(total, norm_ref[1:2, :]).astype(BF16)

    @functools.partial(branches, a, A)
    def drain_heads(me):
        for i in near(me):
            for slot in slots(z.combos[i][0]):
                qkv(me, i, slot).wait_send()

        def drain(other):
            for slot in slots(z.combos[me][0]):
                if slot >= K1:
                    for origin in range(A):
                        kv(me, origin, other, slot).wait_send()

        peers(B, b, drain)

    for kind in (UP, DOWN):
        swap(kind).wait_send()

    @functools.partial(branches, f, F)
    def drain_weights(me):
        for direction in (1, -1):
            if 0 <= me + direction < F:
                for k in range(F):
                    origin = me - direction * k
                    if 0 <= origin < F:
                        for index in range(2):
                            for kind in (UP, DOWN):
                                along(me, origin, index, kind, direction).wait_send()

    peers(n_tp, t, lambda other: [ow_copy(i, other).wait_send() for i in range(A)] and None)
    for n in range(A):
        for other in range(n_tp):
            if n < A - 1:
                outs(n, lax.rem(a + 1 + n, A), other).wait_send()
            else:
                pl.when(t != other)(lambda: outs(n, a, other).wait_send())
    for n in range(z.chips):
        rows_to_pair(n).wait_send()
        half_to_pair(n).wait_send()
        if n:
            rows_to_chip(n).wait_send()
            sum_to_chip(n).wait_send()


def local(
    query_first,
    key_first,
    value_first,
    query_second,
    key_second,
    value_second,
    mix_lambda,
    head_gain,
    out_weight,
    residual,
    norm_gain,
    up_weight,
    down_weight,
    n_sp,
    n_tp,
):
    tokens, heads, width_first = query_first.shape
    width_second = query_second.shape[2]
    value = value_first.shape[2]
    width, hidden = up_weight.shape[0] * n_sp, up_weight.shape[1]
    sub = up_weight.shape[0]
    z = Sizes(n_sp, n_tp, heads, tokens, value, width, sub, hidden)
    half = width_second // 2

    def by_head(array):
        return array.transpose(1, 0, 2)

    def by_map(array):
        return array.reshape(tokens, heads, 2, half).transpose(1, 2, 0, 3)

    lam = jnp.stack([mix_lambda[kind, h] for kind, h in z.combos])
    gains = jnp.stack([head_gain[kind, h] for kind, h in z.combos])
    query_block = next(k for k in (384, 256, 128, tokens) if tokens % k == 0)
    key_block = next(k for k in (1024, 512, 256, tokens) if (n_sp * tokens) % k == 0)
    kernel = functools.partial(
        body, z, (1.0 / math.sqrt(width_first // 2), 1.0 / math.sqrt(half)), query_block, key_block
    )
    total = n_sp * tokens
    rows, A, B, F, chips = z.rows, z.A, z.B, z.F, z.chips
    DMA = pltpu.SemaphoreType.DMA
    vmem = pl.BlockSpec(memory_space=pltpu.VMEM)
    anywhere = pl.BlockSpec(memory_space=pl.ANY)
    return pl.pallas_call(
        kernel,
        in_specs=[pl.BlockSpec(memory_space=pltpu.SMEM), vmem, vmem, vmem] + [anywhere] * 9,
        out_specs=vmem,
        out_shape=jax.ShapeDtypeStruct((rows, width), BF16),
        scratch_shapes=[
            pltpu.VMEM((2, A * tokens, half), BF16),
            pltpu.VMEM((2, total, half), BF16),
            pltpu.VMEM((total, 2 * value), BF16),
            pltpu.VMEM((A * tokens, value), BF16),
            pltpu.VMEM((n_tp * A, rows, value), BF16),
            pltpu.VMEM((n_tp * A * value, width), BF16),
            pltpu.VMEM((width, z.hidden), BF16),
            pltpu.VMEM((n_sp, z.hidden, sub), BF16),
            pltpu.VMEM((2 * chips, rows, width), BF16),
            pltpu.VMEM((rows, width), F32),
            pltpu.VMEM((chips, rows, width), F32),
            pltpu.VMEM((chips, rows, width), BF16),
            pltpu.VMEM((chips, rows, width), BF16),
            pltpu.VMEM((chips, rows, width), BF16),
            pltpu.VMEM((chips, rows, width), BF16),
            DMA((A, 5)),
            DMA((A, 5)),
            DMA((A, B, 3)),
            DMA((A, B, 3)),
            DMA((5,)),
            DMA((2,)),
            DMA((2,)),
            DMA((2, F, 2, 2)),
            DMA((F, 2, 2)),
            DMA((2,)),
            DMA((n_tp, A)),
            DMA((n_tp, A)),
            DMA((A,)),
            DMA((A, n_tp)),
            DMA((n_tp * A,)),
            DMA((chips,)),
            DMA((chips,)),
            DMA((2 * chips,)),
            DMA((chips,)),
            DMA((chips,)),
            DMA((chips,)),
            DMA((chips,)),
        ],
        compiler_params=pltpu.CompilerParams(
            collective_id=0, has_side_effects=True, vmem_limit_bytes=67043328
        ),
    )(
        lam,
        gains,
        norm_gain,
        residual,
        by_head(query_first),
        by_head(key_first),
        by_head(value_first),
        by_map(query_second),
        by_map(key_second),
        by_head(value_second),
        out_weight.reshape(-1, width),
        up_weight,
        down_weight,
    )


def solution(mesh):
    return jax.shard_map(
        functools.partial(local, n_sp=mesh.shape["sp"], n_tp=mesh.shape["tp"]),
        mesh=mesh,
        in_specs=(
            P("sp", "tp", None),
            P("sp", "tp", None),
            P("sp", "tp", None),
            P("sp", "tp", None),
            P("sp", "tp", None),
            P("sp", "tp", None),
            P(None, "tp"),
            P(None, "tp", None),
            P(None, "tp", None, None),
            P(("sp", "tp"), None),
            P(),
            P("sp", "tp"),
            P("tp", "sp"),
        ),
        out_specs=P(("sp", "tp"), None),
        check_vma=False,
    )
```

profile of v0, /device:TPU:25, one launch (start us, length us, event | category | flops | bytes accessed | tf_op | source)
XLA Modules:
  0.0 313.5 jit_solution(7401941616434503480)
XLA Ops:
  0.0 0.0 copy-start
  0.0 1.5 fusion
  1.5 3.2 %pad_maximum_fusion.1.lam_ref = f32[4]{0:T(128)} fusion(f32[1]{0:T(128)} %bitcast.3, f32[1]{0:T(128)} %bitcast.2, f32[1]{0:T(128)} %bitcast.1, f32[1]{0:T(128)} %bitcast), kind=kLoop, calls=%fused_computation.5 | loop fusion | flops 12 | bytes 32 | tf_op jit(solution)/shard_map/stack | solution.py:574
  4.7 0.8 slice_bitcast_fusion.3
  5.4 0.6 pad_maximum_fusion.gain_ref
  6.0 2.2 copy.21
  8.2 0.0 copy-start.1
  8.2 0.0 copy-start.2
  8.3 1.2 copy.22
  9.4 0.0 copy-done
  9.4 0.0 copy-start.3
  9.4 0.0 copy-start.4
  9.4 0.6 copy.23
  10.0 1.2 copy.24
  11.2 0.0 copy-done.1
  11.2 0.0 copy-done.2
  11.2 1.0 copy_bitcast_fusion.2
  12.1 0.0 copy-done.3
  12.2 0.0 copy-done.4
  12.2 1.0 copy_bitcast_fusion
  13.1 298.2 %shard_map.127 = bf16[192,2048]{1,0:T(8,128)(2,1)} custom-call(f32[4]{0:T(128)} %pad_maximum_fusion.1.lam_ref, f32[4,128]{1,0:T(4,128)} %pad_maximum_fusion.gain_ref, f32[2,2048]{1,0:T(2,128)} %norm_ref.1, bf16[192,2048]{1,0:T(8,128)(2,1)} %residual_ref.1, bf16[2,768,128]{2,1,0:T(8,128)(2,1)} %get-tuple-element.16.qf, ...), custom_call_target="tpu_custom_call" | custom-call | tf_op jit(solution)/shard_map/pallas_call | solution.py:586
  311.4 2.1 copy.31
Async XLA Ops:
  0.0 9.4 %copy-start = (bf16[768,2,256]{2,1,0:T(2,128)(2,1)S(1)}, bf16[768,2,256]{2,1,0:T(2,128)(2,1)}, u32[]{:S(2)}) copy-start(bf16[768,2,256]{2,1,0:T(2,128)(2,1)} %param.17) | copy-start | bytes 2359300
  8.2 2.9 copy-start.1
  8.2 2.9 copy-start.2
  9.4 2.7 copy-start.3
  9.4 2.7 copy-start.4
where the time goes:
time: 314 us; the launch traced here: 313 us
  Pallas kernels  298 us (95%)
  local copies, waits for them, and re-layouts  11.4 us (4%)
  other arithmetic  3.78 us (1%)
    pallas_call x1, Pallas kernels, local(): pl.pallas_call(kernel, in_specs=[pl.BlockSpec(memory_space=pltpu.SMEM), v...  298 us

commit v1 on v0

--- a/solution.py
+++ b/solution.py
@@ -80,7 +80,7 @@
     lam_ref,
     gain_ref,
     norm_ref,
-    residual_ref,
+    residual_in,
     qf,
     kf,
     vf,
@@ -101,6 +101,7 @@
     wdn,
     x_all,
     normed_ref,
+    residual_ref,
     own_part,
     s1_out,
     s1_in,
@@ -124,6 +125,9 @@
     x_send,
     xf_send,
     x_recv,
+    xh_send,
+    xh_recv,
+    residual_sem,
     s1_send,
     s1_recv,
     s2_send,
@@ -200,12 +204,16 @@
 
     @functools.partial(branches, a, A)
     def send_heads(me):
-        for i in reversed(near(me)):
-            for slot in reversed(slots(z.combos[i][0])):
-                qkv(me, i, slot).start()
+        for i in near(me):
+            for slot in slots(z.combos[i][0]):
+                if slot >= K1:
+                    qkv(me, i, slot).start()
+        for n in range(1, A):
+            i = (me - n) % A
+            for slot in slots(z.combos[i][0]):
+                if slot < K1:
+                    qkv(me, i, slot).start()
         mine = slots(z.combos[me][0])
-        for slot in mine:
-            qkv_local(me, slot).start()
 
         def share(other):
             for slot in mine:
@@ -213,6 +221,8 @@
                     kv(me, me, other, slot).start()
 
         peers(B, b, share)
+        for slot in mine:
+            qkv_local(me, slot).start()
 
     def wplace(kind, block):
         if kind == UP:
@@ -251,19 +261,25 @@
         @functools.partial(branches, f, F)
         def pass_on(me):
             for k, index, kind in events:
+                if k == 0:
+                    swap_arrival(kind).wait_recv()
                 for direction in (1, -1):
                     origin = me - direction * k
                     if 0 <= origin < F:
-                        move = along(me, origin, index, kind, direction)
-                        move.wait_recv()
+                        if k:
+                            along(me, origin, index, kind, direction).wait_recv()
                         if 0 <= me + direction < F:
-                            move.start()
-
-    events = [(k, index, kind) for k in range(1, F) for index in range(2) for kind in (UP, DOWN)]
+                            along(me, origin, index, kind, direction).start()
+
+    first = [(0, 1, UP), (0, 1, DOWN), (1, 0, UP), (1, 1, UP), (1, 0, DOWN)]
+    rest = [(k, index, UP) for k in range(1, F - 1) for index in range(2)]
+    rest += [(k, index, DOWN) for k in range(1, F - 1) for index in range(2)]
+    events = first + [event for event in rest if event not in first]
+    last = [[(F - 1, index, kind) for index in range(2)] for kind in (UP, DOWN)]
 
     for kind in (UP, DOWN):
-        swap(kind).start()
         wlocal(kind).start()
+    pltpu.make_async_copy(residual_in, residual_ref, residual_sem.at[0]).start()
 
     @functools.partial(branches, f, F)
     def send_own(me):
@@ -309,42 +325,37 @@
             peers(B, b, share)
 
     for kind in (UP, DOWN):
-        swap_arrival(kind).wait_recv()
-
-    @functools.partial(branches, f, F)
-    def send_swapped(me):
-        for kind in (UP, DOWN):
-            for direction in (1, -1):
-                if 0 <= me + direction < F:
-                    along(me, me, 1, kind, direction).start()
+        swap(kind).start()
 
     @functools.partial(branches, a, A)
     def receive_rest(me):
         mine = slots(z.combos[me][0])
         for slot in mine:
             qkv_local(me, slot).wait()
-            if slot < K1:
-                for origin in near(me):
-                    qkv_arrival(origin, slot).wait_recv()
-            else:
+            if slot >= K1:
                 for origin in range(A):
                     peers(B, b, lambda other: kv_arrival(origin, other, slot).wait_recv())
 
     second = sum(jnp.where(a == i, kind, 0) for i, (kind, h) in enumerate(z.combos))
 
-    @when(second == 0)
-    def split_maps():
-        low = lax.broadcasted_iota(jnp.int32, (TD, half), 1) < half // 2
-        for block in range(A):
-            rows = pl.ds(block * TD, TD)
+    def queries_of(origin):
+        @when(origin != a)
+        def arrive():
+            qkv_arrival(origin, Q1).wait_recv()
+            pl.when(second == 1)(lambda: qkv_arrival(origin, Q2).wait_recv())
+
+        @when(second == 0)
+        def split_maps():
+            low = lax.broadcasted_iota(jnp.int32, (TD, half), 1) < half // 2
+            rows = pl.ds(aligned(origin * TD, TD), TD)
             queries = qb[0, rows, :]
             empty = jnp.zeros_like(queries)
             qb[1, rows, :] = jnp.where(low, empty, queries)
             qb[0, rows, :] = jnp.where(low, queries, empty)
 
     factor = jnp.where(second == 0, scales[0], scales[1]) * math.log2(math.e)
-    lam = lam_ref[a]
-    gain = gain_ref[pl.ds(a, 1), :]
+    lam = sum(jnp.where(a == i, lam_ref[kind, h], 0.0) for i, (kind, h) in enumerate(z.combos))
+    gain = sum(jnp.where(a == i, gain_ref[kind, h : h + 1, :], 0.0) for i, (kind, h) in enumerate(z.combos))
 
     def attend(row):
         maxima, sums = [None, None], [None, None]
@@ -381,27 +392,32 @@
         place = gathered.at[index]
         return remote(place, place, o_send.at[0, 0], o_recv.at[index], (s, t))
 
-    early = {0: events[0:2], 1: events[2:3], 2: events[3:4], 3: events[4:6]}
+    blocks = TD // query_block
+    plan = {0: events[0:1], 2: events[1:2], 4: events[2:3], 5: events[3:4], 7: events[4:5]}
+    plan = {point: moves for point, moves in plan.items() if point < A * blocks}
+    pending = [event for event in events if not any(event in moves for moves in plan.values())]
 
     def attention_step(n, carry):
-        owner = lax.rem(a + 1 + n, A)
+        owner = lax.rem(a + n, A)
+        queries_of(owner)
 
         def inner(m, unused):
             attend(owner * TD + m * query_block)
+            for point, moves in plan.items():
+                pl.when(n * blocks + m == point)(functools.partial(relay, moves))
             return unused
 
-        lax.fori_loop(0, TD // query_block, inner, 0)
+        lax.fori_loop(0, blocks, inner, 0)
         for other in range(n_tp):
-            @when((n < A - 1) | (t != other))
+            @when((n > 0) | (t != other))
             def send():
                 outs(n, owner, other).start()
-        for point in range(min(A, len(early))):
-            pl.when(n == point)(functools.partial(relay, early[point]))
         return carry
 
     lax.fori_loop(0, A, attention_step, 0)
     gathered[t * A + a] = head_out[pl.ds(aligned(a * TD + t * R, R), R), :]
-    used = sum(len(early[point]) for point in range(min(A, len(early))))
+    relay(pending[:1])
+    pltpu.make_async_copy(residual_in, residual_ref, residual_sem.at[0]).wait()
 
     for i in range(A):
         ow_local(i).wait()
@@ -437,65 +453,111 @@
         place = x_all.at[index]
         return remote(place, place, x_send.at[0], x_recv.at[index], (s, t))
 
+    def half_rows(n, part, index):
+        place = x_all.at[index, pl.ds(part * (R // 2), R // 2), :]
+        return remote(place, place, xh_send.at[part], xh_recv.at[part], device_of(chip_at(n), core))
+
+    square = z.chips == 4
     rows_to_pair(0).start()
-    for n in range(z.chips - 1, 0, -1):
+    for n in range(1, 3 if square else z.chips):
         rows_to_chip(n).start()
-
-    relay(events[used:])
+    relay(pending[1:2])
+
+    def rows_from_chip(n):
+        index = chip_at(n) * 2 + core
+        if square and n == 3:
+            for part in range(2):
+                half_rows(3, part, index).wait_recv()
+        else:
+            rows_arrival(index).wait_recv()
+        if square and n < 3:
+            half_rows(3 - n, n - 1, index).start()
+        rows_to_pair(n).start()
+
+    for n in range(1, 3 if square else z.chips):
+        rows_from_chip(n)
+    split = max([4] + [1 + i for i, event in enumerate(pending) if event[2] == UP])
+    relay(pending[2:split])
+    relay(last[UP])
     for kind in (UP, DOWN):
         wlocal(kind).wait()
 
-    def half_to_pair(n):
-        return remote(s1_out.at[n], s1_in.at[n], s1_send.at[n], s1_recv.at[n], pair)
-
-    def sum_to_chip(n):
-        return remote(s2_out.at[n], s2_in.at[n], s2_send.at[n], s2_recv.at[n], device_of(chip_at(n), core))
-
-    def feed(n):
+    def expand(n):
         index = chip_at(n)
-        if n:
-            rows_arrival(index * 2 + core).wait_recv()
-            rows_to_pair(n).start()
         rows_arrival(index * 2 + 1 - core).wait_recv()
-        for c in range(2):
-            expanded = jnp.dot(x_all[index * 2 + c], wup[...], preferred_element_type=F32)
-            acted = jnp.square(jnp.maximum(expanded, 0.0)).astype(BF16)
-
-            def columns(block, unused):
-                part = jnp.dot(acted, wdn[block], preferred_element_type=F32)
-                window = pl.ds(aligned(block * sub, sub), sub)
-
-                @when(core == c)
-                def keep():
-                    own_part[n, :, window] = part
-
-                @when(core != c)
-                def give():
-                    s1_out[n, :, window] = part.astype(BF16)
-
-                return unused
-
-            for block in range(n_sp):
-                columns(block, 0)
-        half_to_pair(n).start()
-
-    def reduce(n):
-        half_to_pair(n).wait_recv()
-        s2_out[n] = (own_part[n] + s1_in[n].astype(F32)).astype(BF16)
-        sum_to_chip(n).start()
+        rows = x_all[pl.ds(index * 2, 2)].reshape(2 * R, x_all.shape[2])
+        expanded = jnp.dot(rows, wup[...], preferred_element_type=F32)
+        ow[n * 2 * R : (n + 1) * 2 * R, :hidden] = jnp.square(jnp.maximum(expanded, 0.0)).astype(BF16)
 
     for n in range(z.chips):
-        feed(n)
-        if n > 1:
-            reduce(n - 1)
-    reduce(z.chips - 1)
-
-    half_to_pair(0).wait_recv()
-    total = normed_ref[...] + own_part[0] + s1_in[0].astype(F32)
-    for n in range(1, z.chips):
-        sum_to_chip(n).wait_recv()
-        total = total + s2_in[n].astype(F32)
-    out_ref[...] = layer_norm(total, norm_ref[1:2, :]).astype(BF16)
+        if square and n == 3:
+            rows_from_chip(3)
+        expand(n)
+    relay(pending[split:])
+
+    orders = [sorted(range(F), key=lambda i: abs(i - me)) for me in range(F)]
+    origins = [sum(jnp.where(f == me, orders[me][m], 0) for me in range(F)) for m in range(F)]
+    parts = (range(F - 1), range(F - 1, F))
+
+    def window(part):
+        return pl.ds(parts[part][0], len(parts[part]))
+
+    def half_to_pair(n, part):
+        return remote(
+            s1_out.at[n, window(part)], s1_in.at[n, window(part)], s1_send.at[n, part], s1_recv.at[n, part], pair
+        )
+
+    def sum_to_chip(n, part):
+        return remote(
+            s2_out.at[n, window(part)], s2_in.at[n, window(part)], s2_send.at[n, part], s2_recv.at[n, part],
+            device_of(chip_at(n), core),
+        )
+
+    def contract(n, part):
+        for m in parts[part]:
+            for j in range(GROUP):
+                columns = slice(j * sub, (j + 1) * sub)
+                result = jnp.dot(
+                    ow[n * 2 * R : (n + 1) * 2 * R, :hidden], wdn[origins[m] * GROUP + j], preferred_element_type=F32
+                )
+                for c in range(2):
+                    piece = result[c * R : (c + 1) * R]
+
+                    @when(core == c)
+                    def keep():
+                        own_part[n, m, :, columns] = piece
+
+                    @when(core != c)
+                    def give():
+                        s1_out[n, m, :, columns] = piece.astype(BF16)
+
+        half_to_pair(n, part).start()
+
+    def reduce(n, part):
+        half_to_pair(n, part).wait_recv()
+        for m in parts[part]:
+            s2_out[n, m] = (own_part[n, m] + s1_in[n, m].astype(F32)).astype(BF16)
+        sum_to_chip(n, part).start()
+
+    for part in range(2):
+        if part:
+            relay(last[DOWN])
+        for n in range(z.chips - 1, -1, -1):
+            contract(n, part)
+            if n < z.chips - 1:
+                reduce(n + 1, part)
+
+    for part in range(2):
+        half_to_pair(0, part).wait_recv()
+        for n in range(1, z.chips):
+            sum_to_chip(n, part).wait_recv()
+        for m in parts[part]:
+            columns = pl.ds(aligned(origins[m] * GROUP * sub, GROUP * sub), GROUP * sub)
+            total = normed_ref[:, columns] + own_part[0, m] + s1_in[0, m].astype(F32)
+            for n in range(1, z.chips):
+                total = total + s2_in[n, m].astype(F32)
+            normed_ref[:, columns] = total
+    out_ref[...] = layer_norm(normed_ref[...], norm_ref[1:2, :]).astype(BF16)
 
     @functools.partial(branches, a, A)
     def drain_heads(me):
@@ -528,16 +590,21 @@
     peers(n_tp, t, lambda other: [ow_copy(i, other).wait_send() for i in range(A)] and None)
     for n in range(A):
         for other in range(n_tp):
-            if n < A - 1:
-                outs(n, lax.rem(a + 1 + n, A), other).wait_send()
+            if n:
+                outs(n, lax.rem(a + n, A), other).wait_send()
             else:
                 pl.when(t != other)(lambda: outs(n, a, other).wait_send())
     for n in range(z.chips):
         rows_to_pair(n).wait_send()
-        half_to_pair(n).wait_send()
-        if n:
+        for part in range(2):
+            half_to_pair(n, part).wait_send()
+            if n:
+                sum_to_chip(n, part).wait_send()
+        if n and not (square and n == 3):
             rows_to_chip(n).wait_send()
-            sum_to_chip(n).wait_send()
+    if square:
+        for n in (1, 2):
+            half_rows(3 - n, n - 1, chip_at(n) * 2 + core).wait_send()
 
 
 def local(
@@ -571,8 +638,6 @@
     def by_map(array):
         return array.reshape(tokens, heads, 2, half).transpose(1, 2, 0, 3)
 
-    lam = jnp.stack([mix_lambda[kind, h] for kind, h in z.combos])
-    gains = jnp.stack([head_gain[kind, h] for kind, h in z.combos])
     query_block = next(k for k in (384, 256, 128, tokens) if tokens % k == 0)
     key_block = next(k for k in (1024, 512, 256, tokens) if (n_sp * tokens) % k == 0)
     kernel = functools.partial(
@@ -585,7 +650,7 @@
     anywhere = pl.BlockSpec(memory_space=pl.ANY)
     return pl.pallas_call(
         kernel,
-        in_specs=[pl.BlockSpec(memory_space=pltpu.SMEM), vmem, vmem, vmem] + [anywhere] * 9,
+        in_specs=[pl.BlockSpec(memory_space=pltpu.SMEM), vmem, vmem] + [anywhere] * 10,
         out_specs=vmem,
         out_shape=jax.ShapeDtypeStruct((rows, width), BF16),
         scratch_shapes=[
@@ -599,11 +664,12 @@
             pltpu.VMEM((n_sp, z.hidden, sub), BF16),
             pltpu.VMEM((2 * chips, rows, width), BF16),
             pltpu.VMEM((rows, width), F32),
-            pltpu.VMEM((chips, rows, width), F32),
-            pltpu.VMEM((chips, rows, width), BF16),
-            pltpu.VMEM((chips, rows, width), BF16),
-            pltpu.VMEM((chips, rows, width), BF16),
-            pltpu.VMEM((chips, rows, width), BF16),
+            pltpu.VMEM((rows, width), BF16),
+            pltpu.VMEM((chips, F, rows, GROUP * sub), F32),
+            pltpu.VMEM((chips, F, rows, GROUP * sub), BF16),
+            pltpu.VMEM((chips, F, rows, GROUP * sub), BF16),
+            pltpu.VMEM((chips, F, rows, GROUP * sub), BF16),
+            pltpu.VMEM((chips, F, rows, GROUP * sub), BF16),
             DMA((A, 5)),
             DMA((A, 5)),
             DMA((A, B, 3)),
@@ -622,17 +688,20 @@
             DMA((chips,)),
             DMA((chips,)),
             DMA((2 * chips,)),
-            DMA((chips,)),
-            DMA((chips,)),
-            DMA((chips,)),
-            DMA((chips,)),
+            DMA((2,)),
+            DMA((2,)),
+            DMA((1,)),
+            DMA((chips, 2)),
+            DMA((chips, 2)),
+            DMA((chips, 2)),
+            DMA((chips, 2)),
         ],
         compiler_params=pltpu.CompilerParams(
             collective_id=0, has_side_effects=True, vmem_limit_bytes=67043328
         ),
     )(
-        lam,
-        gains,
+        mix_lambda,
+        head_gain,
         norm_gain,
         residual,
         by_head(query_first),

time: 314 us -> 264 us (0.84)
  the two profiles are of different devices: /device:TPU:25 before, /device:TPU:0 now
where the time goes in v1:
time: 264 us
  Pallas kernels  255 us (97%)
  local copies, waits for them, and re-layouts  9.29 us (4%)
    pallas_call x1, Pallas kernels, local(): pl.pallas_call(kernel, in_specs=[pl.BlockSpec(memory_space=pltpu.SMEM), v...  255 us

profile of v1, /device:TPU:0, one launch (start us, length us, event | category | flops | bytes accessed | tf_op | source)
XLA Modules:
  0.0 263.9 jit_solution(17072687589834919635)
XLA Ops:
  0.0 0.0 copy-start
  0.0 2.3 copy.21
  2.3 0.0 copy-start.1
  2.3 0.0 copy-start.2
  2.3 1.2 copy.22
  3.5 0.0 copy-done
  3.5 0.0 copy-start.3
  3.5 0.0 copy-start.4
  3.5 0.6 copy.23
  4.1 1.2 copy.24
  5.2 0.0 copy-done.1
  5.2 0.0 copy-done.2
  5.2 1.0 copy_bitcast_fusion.2
  6.2 0.0 copy-done.3
  6.2 0.0 copy-done.4
  6.2 1.0 copy_bitcast_fusion
  7.2 254.5 %shard_map.127 = bf16[192,2048]{1,0:T(8,128)(2,1)} custom-call(f32[2,2]{1,0:T(2,128)} %lam_ref.1, f32[2,2,128]{2,1,0:T(2,128)} %gain_ref.1, f32[2,2048]{1,0:T(2,128)} %norm_ref.1, bf16[192,2048]{1,0:T(8,128)(2,1)} %residual_in.1, bf16[2,768,128]{2,1,0:T(8,128)(2,1)} %get-tuple-element.8.qf, bf16[2,768,128]{2,1,0:T(8,128)(2,1)} %get-tuple-element.7.kf, ...), custom_call_target="tpu_custom_call" | custom-call | tf_op jit(solution)/shard_map/pallas_call | solution.py:651
  261.8 2.1 copy.31
Async XLA Ops:
  0.0 3.5 %copy-start = (bf16[768,2,256]{2,1,0:T(2,128)(2,1)S(1)}, bf16[768,2,256]{2,1,0:T(2,128)(2,1)}, u32[]{:S(2)}) copy-start(bf16[768,2,256]{2,1,0:T(2,128)(2,1)} %param.17) | copy-start | bytes 2359300
  2.3 2.9 %copy-start.1 = (bf16[768,2,128]{2,1,0:T(2,128)(2,1)S(1)}, bf16[768,2,128]{2,1,0:T(2,128)(2,1)}, u32[]{:S(2)}) copy-start(bf16[768,2,128]{2,1,0:T(2,128)(2,1)} %param.14) | copy-start | bytes 1179652
  2.3 2.9 %copy-start.2 = (bf16[768,2,128]{2,1,0:T(2,128)(2,1)S(1)}, bf16[768,2,128]{2,1,0:T(2,128)(2,1)}, u32[]{:S(2)}) copy-start(bf16[768,2,128]{2,1,0:T(2,128)(2,1)} %param.13) | copy-start | bytes 1179652
  3.5 2.8 %copy-start.3 = (bf16[768,2,128]{2,1,0:T(2,128)(2,1)S(1)}, bf16[768,2,128]{2,1,0:T(2,128)(2,1)}, u32[]{:S(2)}) copy-start(bf16[768,2,128]{2,1,0:T(2,128)(2,1)} %param.18) | copy-start | bytes 1179652
  3.5 2.8 %copy-start.4 = (bf16[768,2,128]{2,1,0:T(2,128)(2,1)S(1)}, bf16[768,2,128]{2,1,0:T(2,128)(2,1)}, u32[]{:S(2)}) copy-start(bf16[768,2,128]{2,1,0:T(2,128)(2,1)} %param.15) | copy-start | bytes 1179652

commit v2 on v1

--- a/solution.py
+++ b/solution.py
@@ -102,11 +102,11 @@
     x_all,
     normed_ref,
     residual_ref,
-    own_part,
-    s1_out,
+    partial,
     s1_in,
     s2_out,
     s2_in,
+    sh_in,
     qkv_send,
     qkv_recv,
     kv_send,
@@ -132,6 +132,8 @@
     s1_recv,
     s2_send,
     s2_recv,
+    sh_send,
+    sh_recv,
 ):
     s, t = lax.axis_index("sp"), lax.axis_index("tp")
     A, B, F, n_sp, n_tp = z.A, z.B, z.F, z.n_sp, z.n_tp
@@ -199,6 +201,9 @@
         for k in range(count):
             pl.when(mine != k)(functools.partial(action, k))
 
+    def visits(me):
+        return [me] + sorted((i for i in range(A) if i != me), key=lambda i: (-abs(2 * i - A + 1), -abs(i - me)))
+
     def near(me):
         return sorted((i for i in range(A) if i != me), key=lambda i: abs(i - me))
 
@@ -208,11 +213,6 @@
             for slot in slots(z.combos[i][0]):
                 if slot >= K1:
                     qkv(me, i, slot).start()
-        for n in range(1, A):
-            i = (me - n) % A
-            for slot in slots(z.combos[i][0]):
-                if slot < K1:
-                    qkv(me, i, slot).start()
         mine = slots(z.combos[me][0])
 
         def share(other):
@@ -227,7 +227,7 @@
     def wplace(kind, block):
         if kind == UP:
             return wup.at[pl.ds(aligned(block * sub, sub), sub), :]
-        return wdn.at[block]
+        return wdn.at[lax.div(block, GROUP), :, pl.ds(aligned(lax.rem(block, GROUP) * sub, sub), sub)]
 
     def wsource(kind, half):
         window = pl.ds(aligned(half * hidden, hidden), hidden)
@@ -254,39 +254,45 @@
             ((me + direction) * GROUP + g, t),
         )
 
-    def relay(events):
-        if not events:
+    def crossing(me, direction):
+        return (me < F // 2) != (me + direction < F // 2)
+
+    def send_own(index, kind, crossings=(False, True)):
+        @functools.partial(branches, f, F)
+        def send(me):
+            for direction in (1, -1):
+                if 0 <= me + direction < F and crossing(me, direction) in crossings:
+                    along(me, me, index, kind, direction, raw=index == 0).start()
+
+    def relay(moves, ways=("in", "out"), forward=True):
+        if not moves:
             return
 
         @functools.partial(branches, f, F)
         def pass_on(me):
-            for k, index, kind in events:
-                if k == 0:
-                    swap_arrival(kind).wait_recv()
+            for k, index, kind in moves:
                 for direction in (1, -1):
                     origin = me - direction * k
-                    if 0 <= origin < F:
-                        if k:
-                            along(me, origin, index, kind, direction).wait_recv()
-                        if 0 <= me + direction < F:
+                    way = "out" if direction == (1 if me >= F // 2 else -1) else "in"
+                    onward = 0 <= me + direction < F
+                    if 0 <= origin < F and way in ways and onward == forward:
+                        along(me, origin, index, kind, direction).wait_recv()
+                        if onward:
                             along(me, origin, index, kind, direction).start()
 
-    first = [(0, 1, UP), (0, 1, DOWN), (1, 0, UP), (1, 1, UP), (1, 0, DOWN)]
-    rest = [(k, index, UP) for k in range(1, F - 1) for index in range(2)]
-    rest += [(k, index, DOWN) for k in range(1, F - 1) for index in range(2)]
-    events = first + [event for event in rest if event not in first]
-    last = [[(F - 1, index, kind) for index in range(2)] for kind in (UP, DOWN)]
+    def settle(low, high, kind):
+        relay(chunks(low, high, kind), forward=False)
+
+    def chunks(low, high, kind):
+        return [(k, index, kind) for k in range(low, high) for index in range(2)]
+
+    ups = chunks(1, F - 1, UP)
+    downs, downs_near, downs_far = chunks(1, F - 1, DOWN), chunks(1, F // 2, DOWN), chunks(F // 2, F - 1, DOWN)
 
     for kind in (UP, DOWN):
+        send_own(0, kind, (False,))
         wlocal(kind).start()
     pltpu.make_async_copy(residual_in, residual_ref, residual_sem.at[0]).start()
-
-    @functools.partial(branches, f, F)
-    def send_own(me):
-        for kind in (UP, DOWN):
-            for direction in (1, -1):
-                if 0 <= me + direction < F:
-                    along(me, me, 0, kind, direction, raw=True).start()
 
     def ow_rows(i):
         kind, h = z.combos[i]
@@ -324,8 +330,16 @@
 
             peers(B, b, share)
 
+    @functools.partial(branches, a, A)
+    def send_queries(me):
+        for i in sorted(near(me), key=lambda i: visits(i).index(me)):
+            for slot in slots(z.combos[i][0]):
+                if slot < K1:
+                    qkv(me, i, slot).start()
+
     for kind in (UP, DOWN):
         swap(kind).start()
+    send_own(0, UP, (True,))
 
     @functools.partial(branches, a, A)
     def receive_rest(me):
@@ -393,18 +407,29 @@
         return remote(place, place, o_send.at[0, 0], o_recv.at[index], (s, t))
 
     blocks = TD // query_block
-    plan = {0: events[0:1], 2: events[1:2], 4: events[2:3], 5: events[3:4], 7: events[4:5]}
-    plan = {point: moves for point, moves in plan.items() if point < A * blocks}
-    pending = [event for event in events if not any(event in moves for moves in plan.values())]
-
+
+    def own_up():
+        swap_arrival(UP).wait_recv()
+        send_own(1, UP)
+
+    def own_down():
+        swap_arrival(DOWN).wait_recv()
+        send_own(1, DOWN, (False,))
+
+    plan = {2: own_up, 3: own_down}
+    for point, move in zip((4, 6), ups):
+        plan[point] = functools.partial(relay, [move])
     def attention_step(n, carry):
-        owner = lax.rem(a + n, A)
+        owner = sum(
+            jnp.where((a == me) & (n == k), i, 0) for me in range(A) for k, i in enumerate(visits(me))
+        )
         queries_of(owner)
 
         def inner(m, unused):
             attend(owner * TD + m * query_block)
-            for point, moves in plan.items():
-                pl.when(n * blocks + m == point)(functools.partial(relay, moves))
+            for point, action in plan.items():
+                if point < A * blocks:
+                    pl.when(n * blocks + m == point)(action)
             return unused
 
         lax.fori_loop(0, blocks, inner, 0)
@@ -416,7 +441,13 @@
 
     lax.fori_loop(0, A, attention_step, 0)
     gathered[t * A + a] = head_out[pl.ds(aligned(a * TD + t * R, R), R), :]
-    relay(pending[:1])
+    for point, action in plan.items():
+        if point >= A * blocks:
+            action()
+    send_own(0, DOWN, (True,))
+    send_own(1, DOWN, (True,))
+    relay(downs, ("in",))
+    relay(ups[2:3])
     pltpu.make_async_copy(residual_in, residual_ref, residual_sem.at[0]).wait()
 
     for i in range(A):
@@ -461,7 +492,7 @@
     rows_to_pair(0).start()
     for n in range(1, 3 if square else z.chips):
         rows_to_chip(n).start()
-    relay(pending[1:2])
+    relay(ups[3:4])
 
     def rows_from_chip(n):
         index = chip_at(n) * 2 + core
@@ -476,9 +507,9 @@
 
     for n in range(1, 3 if square else z.chips):
         rows_from_chip(n)
-    split = max([4] + [1 + i for i, event in enumerate(pending) if event[2] == UP])
-    relay(pending[2:split])
-    relay(last[UP])
+        relay(downs_near[:1] if n == 1 else downs_near[1:] if n == 2 else [], ("out",))
+    relay(ups[4:])
+    settle(1, F, UP)
     for kind in (UP, DOWN):
         wlocal(kind).wait()
 
@@ -493,18 +524,20 @@
         if square and n == 3:
             rows_from_chip(3)
         expand(n)
-    relay(pending[split:])
-
-    orders = [sorted(range(F), key=lambda i: abs(i - me)) for me in range(F)]
+        relay(downs_far[:1] if n == 0 else downs_far[1:] if n == 1 else [], ("out",))
+
+    orders = [sorted(range(F), key=lambda i: (F * ((i < F // 2) != (me < F // 2)) + abs(i - me))) for me in range(F)]
     origins = [sum(jnp.where(f == me, orders[me][m], 0) for me in range(F)) for m in range(F)]
-    parts = (range(F - 1), range(F - 1, F))
+    limits = (0, F // 2, F - 1, F)
+    parts = [range(low, high) for low, high in zip(limits, limits[1:]) if low < high]
 
     def window(part):
         return pl.ds(parts[part][0], len(parts[part]))
 
     def half_to_pair(n, part):
         return remote(
-            s1_out.at[n, window(part)], s1_in.at[n, window(part)], s1_send.at[n, part], s1_recv.at[n, part], pair
+            partial.at[n, 1 - core, window(part)], s1_in.at[n, window(part)], s1_send.at[n, part],
+            s1_recv.at[n, part], pair,
         )
 
     def sum_to_chip(n, part):
@@ -513,48 +546,58 @@
             device_of(chip_at(n), core),
         )
 
+    def half_sum(way, part):
+        return remote(
+            s2_out.at[3, window(part), pl.ds((way - 1) * (R // 2), R // 2), :], sh_in.at[way, window(part)],
+            sh_send.at[way, part], sh_recv.at[way, part], device_of(chip_at(way), core),
+        )
+
     def contract(n, part):
         for m in parts[part]:
-            for j in range(GROUP):
-                columns = slice(j * sub, (j + 1) * sub)
-                result = jnp.dot(
-                    ow[n * 2 * R : (n + 1) * 2 * R, :hidden], wdn[origins[m] * GROUP + j], preferred_element_type=F32
-                )
-                for c in range(2):
-                    piece = result[c * R : (c + 1) * R]
-
-                    @when(core == c)
-                    def keep():
-                        own_part[n, m, :, columns] = piece
-
-                    @when(core != c)
-                    def give():
-                        s1_out[n, m, :, columns] = piece.astype(BF16)
-
+            result = jnp.dot(
+                ow[n * 2 * R : (n + 1) * 2 * R, :hidden], wdn[origins[m]], preferred_element_type=F32
+            ).astype(BF16)
+            for c in range(2):
+                partial[n, c, m] = result[c * R : (c + 1) * R]
         half_to_pair(n, part).start()
 
     def reduce(n, part):
         half_to_pair(n, part).wait_recv()
+        way = 3 - n
+        if square and n < 3:
+            half_sum(way, part).wait_recv()
         for m in parts[part]:
-            s2_out[n, m] = (own_part[n, m] + s1_in[n, m].astype(F32)).astype(BF16)
-        sum_to_chip(n, part).start()
-
-    for part in range(2):
-        if part:
-            relay(last[DOWN])
-        for n in range(z.chips - 1, -1, -1):
+            added = partial[n, core, m].astype(F32) + s1_in[n, m].astype(F32)
+            if square and n < 3:
+                passing = sh_in[way, m].astype(F32)
+                empty = jnp.zeros_like(passing)
+                added += jnp.concatenate([passing, empty] if way == 1 else [empty, passing])
+            s2_out[n, m] = added.astype(BF16)
+        if square and n == 3:
+            for other in (1, 2):
+                half_sum(other, part).start()
+        else:
+            sum_to_chip(n, part).start()
+
+    order = list(range(z.chips - 1, -1, -1))
+    for part in range(len(parts)):
+        settle(max(1, parts[part][0]), parts[part][-1] + 1, DOWN)
+        for step, n in enumerate(order):
             contract(n, part)
-            if n < z.chips - 1:
-                reduce(n + 1, part)
-
-    for part in range(2):
+            if step == 1:
+                reduce(order[0], part)
+        for n in order[1:-1]:
+            reduce(n, part)
+
+    senders = range(1, 3 if square else z.chips)
+    for part in range(len(parts)):
         half_to_pair(0, part).wait_recv()
-        for n in range(1, z.chips):
+        for n in senders:
             sum_to_chip(n, part).wait_recv()
         for m in parts[part]:
             columns = pl.ds(aligned(origins[m] * GROUP * sub, GROUP * sub), GROUP * sub)
-            total = normed_ref[:, columns] + own_part[0, m] + s1_in[0, m].astype(F32)
-            for n in range(1, z.chips):
+            total = normed_ref[:, columns] + partial[0, core, m].astype(F32) + s1_in[0, m].astype(F32)
+            for n in senders:
                 total = total + s2_in[n, m].astype(F32)
             normed_ref[:, columns] = total
     out_ref[...] = layer_norm(normed_ref[...], norm_ref[1:2, :]).astype(BF16)
@@ -591,20 +634,22 @@
     for n in range(A):
         for other in range(n_tp):
             if n:
-                outs(n, lax.rem(a + n, A), other).wait_send()
+                outs(n, a, other).wait_send()
             else:
                 pl.when(t != other)(lambda: outs(n, a, other).wait_send())
     for n in range(z.chips):
         rows_to_pair(n).wait_send()
-        for part in range(2):
+        for part in range(len(parts)):
             half_to_pair(n, part).wait_send()
-            if n:
+            if n in senders:
                 sum_to_chip(n, part).wait_send()
         if n and not (square and n == 3):
             rows_to_chip(n).wait_send()
     if square:
         for n in (1, 2):
             half_rows(3 - n, n - 1, chip_at(n) * 2 + core).wait_send()
+            for part in range(len(parts)):
+                half_sum(n, part).wait_send()
 
 
 def local(
@@ -661,15 +706,15 @@
             pltpu.VMEM((n_tp * A, rows, value), BF16),
             pltpu.VMEM((n_tp * A * value, width), BF16),
             pltpu.VMEM((width, z.hidden), BF16),
-            pltpu.VMEM((n_sp, z.hidden, sub), BF16),
+            pltpu.VMEM((F, z.hidden, GROUP * sub), BF16),
             pltpu.VMEM((2 * chips, rows, width), BF16),
             pltpu.VMEM((rows, width), F32),
             pltpu.VMEM((rows, width), BF16),
-            pltpu.VMEM((chips, F, rows, GROUP * sub), F32),
+            pltpu.VMEM((chips, 2, F, rows, GROUP * sub), BF16),
             pltpu.VMEM((chips, F, rows, GROUP * sub), BF16),
             pltpu.VMEM((chips, F, rows, GROUP * sub), BF16),
             pltpu.VMEM((chips, F, rows, GROUP * sub), BF16),
-            pltpu.VMEM((chips, F, rows, GROUP * sub), BF16),
+            pltpu.VMEM((3, F, rows // 2, GROUP * sub), BF16),
             DMA((A, 5)),
             DMA((A, 5)),
             DMA((A, B, 3)),
@@ -691,10 +736,12 @@
             DMA((2,)),
             DMA((2,)),
             DMA((1,)),
-            DMA((chips, 2)),
-            DMA((chips, 2)),
-            DMA((chips, 2)),
-            DMA((chips, 2)),
+            DMA((chips, 3)),
+            DMA((chips, 3)),
+            DMA((chips, 3)),
+            DMA((chips, 3)),
+            DMA((3, 3)),
+            DMA((3, 3)),
         ],
         compiler_params=pltpu.CompilerParams(
             collective_id=0, has_side_effects=True, vmem_limit_bytes=67043328

time: 264 us -> 234 us (0.89)
  Pallas kernels: 255 us -> 224 us
    pallas_call x1, Pallas kernels: 255 us -> 224 us  [local(): pl.pallas_call(kernel, in_specs=[pl.BlockSpec(memory_space=pltpu.SMEM), v...]
where the time goes in v2:
time: 234 us; the launch traced here: 233 us
  Pallas kernels  224 us (96%)
  local copies, waits for them, and re-layouts  9.29 us (4%)
    pallas_call x1, Pallas kernels, local(): pl.pallas_call(kernel, in_specs=[pl.BlockSpec(memory_space=pltpu.SMEM), v...  224 us
    unnamed x13, local copies, waits for them, and re-layouts  4.98 us

profile of v2, /device:TPU:0, one launch (start us, length us, event | category | flops | bytes accessed | tf_op | source)
XLA Modules:
  0.0 233.1 jit_solution(14076284175798519613)
XLA Ops:
  0.0 0.0 copy-start
  0.0 2.3 copy.21
  2.3 0.0 copy-start.1
  2.3 0.0 copy-start.2
  2.3 1.2 copy.22
  3.5 0.0 copy-done
  3.5 0.0 copy-start.3
  3.5 0.0 copy-start.4
  3.5 0.6 copy.23
  4.1 1.2 copy.24
  5.2 0.0 copy-done.1
  5.2 0.0 copy-done.2
  5.2 1.0 copy_bitcast_fusion.2
  6.2 0.0 copy-done.3
  6.2 0.0 copy-done.4
  6.2 1.0 copy_bitcast_fusion
  7.2 223.8 %shard_map.127 = bf16[192,2048]{1,0:T(8,128)(2,1)} custom-call(f32[2,2]{1,0:T(2,128)} %lam_ref.1, f32[2,2,128]{2,1,0:T(2,128)} %gain_ref.1, f32[2,2048]{1,0:T(2,128)} %norm_ref.1, bf16[192,2048]{1,0:T(8,128)(2,1)} %residual_in.1, bf16[2,768,128]{2,1,0:T(8,128)(2,1)} %get-tuple-element.8.qf, bf16[2,768,128]{2,1,0:T(8,128)(2,1)} %get-tuple-element.7.kf, ...), custom_call_target="tpu_custom_call" | custom-call | tf_op jit(solution)/shard_map/pallas_call | solution.py:696
  231.0 2.1 copy.31
Async XLA Ops:
  0.0 3.5 %copy-start = (bf16[768,2,256]{2,1,0:T(2,128)(2,1)S(1)}, bf16[768,2,256]{2,1,0:T(2,128)(2,1)}, u32[]{:S(2)}) copy-start(bf16[768,2,256]{2,1,0:T(2,128)(2,1)} %param.17) | copy-start | bytes 2359300
  2.3 2.9 %copy-start.1 = (bf16[768,2,128]{2,1,0:T(2,128)(2,1)S(1)}, bf16[768,2,128]{2,1,0:T(2,128)(2,1)}, u32[]{:S(2)}) copy-start(bf16[768,2,128]{2,1,0:T(2,128)(2,1)} %param.14) | copy-start | bytes 1179652
  2.3 2.9 %copy-start.2 = (bf16[768,2,128]{2,1,0:T(2,128)(2,1)S(1)}, bf16[768,2,128]{2,1,0:T(2,128)(2,1)}, u32[]{:S(2)}) copy-start(bf16[768,2,128]{2,1,0:T(2,128)(2,1)} %param.13) | copy-start | bytes 1179652
  3.5 2.8 %copy-start.3 = (bf16[768,2,128]{2,1,0:T(2,128)(2,1)S(1)}, bf16[768,2,128]{2,1,0:T(2,128)(2,1)}, u32[]{:S(2)}) copy-start(bf16[768,2,128]{2,1,0:T(2,128)(2,1)} %param.18) | copy-start | bytes 1179652
  3.5 2.8 %copy-start.4 = (bf16[768,2,128]{2,1,0:T(2,128)(2,1)S(1)}, bf16[768,2,128]{2,1,0:T(2,128)(2,1)}, u32[]{:S(2)}) copy-start(bf16[768,2,128]{2,1,0:T(2,128)(2,1)} %param.15) | copy-start | bytes 1179652

commit v3 on v2

--- a/solution.py
+++ b/solution.py
@@ -245,8 +245,10 @@
     def wlocal(kind):
         return pltpu.make_async_copy(wsource(kind, g), wplace(kind, s), wlocal_sem.at[kind])
 
-    def along(me, origin, index, kind, direction, raw=False):
+    def along(me, origin, index, kind, direction, raw=False, fixed=False):
         j = g if index == 0 else 1 - g
+        if fixed:
+            j, index = index, lax.rem(index + g, 2)
         place = wplace(kind, origin * GROUP + j)
         src = wsource(kind, g) if raw else place
         return remote(
@@ -257,12 +259,12 @@
     def crossing(me, direction):
         return (me < F // 2) != (me + direction < F // 2)
 
-    def send_own(index, kind, crossings=(False, True)):
+    def send_own(index, kind, crossings=(False, True), fixed=False):
         @functools.partial(branches, f, F)
         def send(me):
             for direction in (1, -1):
                 if 0 <= me + direction < F and crossing(me, direction) in crossings:
-                    along(me, me, index, kind, direction, raw=index == 0).start()
+                    along(me, me, index, kind, direction, index == 0 and not fixed, fixed).start()
 
     def relay(moves, ways=("in", "out"), forward=True):
         if not moves:
@@ -276,9 +278,9 @@
                     way = "out" if direction == (1 if me >= F // 2 else -1) else "in"
                     onward = 0 <= me + direction < F
                     if 0 <= origin < F and way in ways and onward == forward:
-                        along(me, origin, index, kind, direction).wait_recv()
+                        along(me, origin, index, kind, direction, fixed=kind == DOWN).wait_recv()
                         if onward:
-                            along(me, origin, index, kind, direction).start()
+                            along(me, origin, index, kind, direction, fixed=kind == DOWN).start()
 
     def settle(low, high, kind):
         relay(chunks(low, high, kind), forward=False)
@@ -337,8 +339,13 @@
                 if slot < K1:
                     qkv(me, i, slot).start()
 
-    for kind in (UP, DOWN):
-        swap(kind).start()
+    at_end = (f == 0) | (f == F - 1)
+
+    def swap_weights():
+        for kind in (UP, DOWN):
+            swap(kind).start()
+
+    pl.when(jnp.logical_not(at_end))(swap_weights)
     send_own(0, UP, (True,))
 
     @functools.partial(branches, a, A)
@@ -350,6 +357,9 @@
                 for origin in range(A):
                     peers(B, b, lambda other: kv_arrival(origin, other, slot).wait_recv())
 
+    pl.when(at_end)(swap_weights)
+    for kind in (UP, DOWN):
+        wlocal(kind).wait()
     second = sum(jnp.where(a == i, kind, 0) for i, (kind, h) in enumerate(z.combos))
 
     def queries_of(origin):
@@ -416,7 +426,7 @@
         swap_arrival(DOWN).wait_recv()
         send_own(1, DOWN, (False,))
 
-    plan = {2: own_up, 3: own_down}
+    plan = {1: own_up, 3: own_down}
     for point, move in zip((4, 6), ups):
         plan[point] = functools.partial(relay, [move])
     def attention_step(n, carry):
@@ -444,8 +454,8 @@
     for point, action in plan.items():
         if point >= A * blocks:
             action()
-    send_own(0, DOWN, (True,))
-    send_own(1, DOWN, (True,))
+    send_own(0, DOWN, (True,), True)
+    send_own(1, DOWN, (True,), True)
     relay(downs, ("in",))
     relay(ups[2:3])
     pltpu.make_async_copy(residual_in, residual_ref, residual_sem.at[0]).wait()
@@ -510,8 +520,6 @@
         relay(downs_near[:1] if n == 1 else downs_near[1:] if n == 2 else [], ("out",))
     relay(ups[4:])
     settle(1, F, UP)
-    for kind in (UP, DOWN):
-        wlocal(kind).wait()
 
     def expand(n):
         index = chip_at(n)
@@ -524,11 +532,11 @@
         if square and n == 3:
             rows_from_chip(3)
         expand(n)
-        relay(downs_far[:1] if n == 0 else downs_far[1:] if n == 1 else [], ("out",))
+        relay(downs_far[:1] if n == 2 else [], ("out",))
 
     orders = [sorted(range(F), key=lambda i: (F * ((i < F // 2) != (me < F // 2)) + abs(i - me))) for me in range(F)]
     origins = [sum(jnp.where(f == me, orders[me][m], 0) for me in range(F)) for m in range(F)]
-    limits = (0, F // 2, F - 1, F)
+    limits = (0, F, 2 * F - 2, 2 * F - 1, 2 * F)
     parts = [range(low, high) for low, high in zip(limits, limits[1:]) if low < high]
 
     def window(part):
@@ -553,12 +561,19 @@
         )
 
     def contract(n, part):
-        for m in parts[part]:
+        units = list(parts[part])
+        while units:
+            paired = len(units) > 1
+            unit = units[0]
+            columns = slice(0, 2 * sub) if paired else slice(unit % 2 * sub, (unit % 2 + 1) * sub)
             result = jnp.dot(
-                ow[n * 2 * R : (n + 1) * 2 * R, :hidden], wdn[origins[m]], preferred_element_type=F32
+                ow[n * 2 * R : (n + 1) * 2 * R, :hidden], wdn[origins[unit // 2], :, columns],
+                preferred_element_type=F32,
             ).astype(BF16)
             for c in range(2):
-                partial[n, c, m] = result[c * R : (c + 1) * R]
+                for j in range(1 + paired):
+                    partial[n, c, unit + j] = result[c * R : (c + 1) * R, j * sub : (j + 1) * sub]
+            units = units[1 + paired :]
         half_to_pair(n, part).start()
 
     def reduce(n, part):
@@ -581,11 +596,16 @@
 
     order = list(range(z.chips - 1, -1, -1))
     for part in range(len(parts)):
-        settle(max(1, parts[part][0]), parts[part][-1] + 1, DOWN)
+        last = parts[part][-1] // 2
+        if len(parts[part]) > 1:
+            settle(max(1, parts[part][0] // 2), last + 1, DOWN)
+        else:
+            relay([(last, parts[part][0] % 2, DOWN)], forward=False)
         for step, n in enumerate(order):
             contract(n, part)
             if step == 1:
                 reduce(order[0], part)
+                relay([] if part else downs_far[1:], ("out",))
         for n in order[1:-1]:
             reduce(n, part)
 
@@ -595,7 +615,7 @@
         for n in senders:
             sum_to_chip(n, part).wait_recv()
         for m in parts[part]:
-            columns = pl.ds(aligned(origins[m] * GROUP * sub, GROUP * sub), GROUP * sub)
+            columns = pl.ds(aligned((origins[m // 2] * GROUP + m % 2) * sub, sub), sub)
             total = normed_ref[:, columns] + partial[0, core, m].astype(F32) + s1_in[0, m].astype(F32)
             for n in senders:
                 total = total + s2_in[n, m].astype(F32)
@@ -710,11 +730,11 @@
             pltpu.VMEM((2 * chips, rows, width), BF16),
             pltpu.VMEM((rows, width), F32),
             pltpu.VMEM((rows, width), BF16),
-            pltpu.VMEM((chips, 2, F, rows, GROUP * sub), BF16),
-            pltpu.VMEM((chips, F, rows, GROUP * sub), BF16),
-            pltpu.VMEM((chips, F, rows, GROUP * sub), BF16),
-            pltpu.VMEM((chips, F, rows, GROUP * sub), BF16),
-            pltpu.VMEM((3, F, rows // 2, GROUP * sub), BF16),
+            pltpu.VMEM((chips, 2, n_sp, rows, sub), BF16),
+            pltpu.VMEM((chips, n_sp, rows, sub), BF16),
+            pltpu.VMEM((chips, n_sp, rows, sub), BF16),
+            pltpu.VMEM((chips, n_sp, rows, sub), BF16),
+            pltpu.VMEM((3, n_sp, rows // 2, sub), BF16),
             DMA((A, 5)),
             DMA((A, 5)),
             DMA((A, B, 3)),
@@ -736,12 +756,12 @@
             DMA((2,)),
             DMA((2,)),
             DMA((1,)),
-            DMA((chips, 3)),
-            DMA((chips, 3)),
-            DMA((chips, 3)),
-            DMA((chips, 3)),
-            DMA((3, 3)),
-            DMA((3, 3)),
+            DMA((chips, 4)),
+            DMA((chips, 4)),
+            DMA((chips, 4)),
+            DMA((chips, 4)),
+            DMA((3, 4)),
+            DMA((3, 4)),
         ],
         compiler_params=pltpu.CompilerParams(
             collective_id=0, has_side_effects=True, vmem_limit_bytes=67043328

time: 234 us -> 230 us (0.983)
  Pallas kernels: 224 us -> 221 us
    pallas_call x1, Pallas kernels: 224 us -> 221 us  [local(): pl.pallas_call(kernel, in_specs=[pl.BlockSpec(memory_space=pltpu.SMEM), v...]
where the time goes in v3:
time: 230 us
  Pallas kernels  221 us (96%)
  local copies, waits for them, and re-layouts  9.29 us (4%)
    pallas_call x1, Pallas kernels, local(): pl.pallas_call(kernel, in_specs=[pl.BlockSpec(memory_space=pltpu.SMEM), v...  221 us
    unnamed x13, local copies, waits for them, and re-layouts  4.98 us

profile of v3, /device:TPU:0, one launch (start us, length us, event | category | flops | bytes accessed | tf_op | source)
XLA Modules:
  0.0 230.1 jit_solution(15243318727715378406)
XLA Ops:
  0.0 0.0 copy-start
  0.0 2.3 copy.21
  2.3 0.0 copy-start.1
  2.3 0.0 copy-start.2
  2.3 1.2 copy.22
  3.5 0.0 copy-done
  3.5 0.0 copy-start.3
  3.5 0.0 copy-start.4
  3.5 0.6 copy.23
  4.1 1.2 copy.24
  5.2 0.0 copy-done.1
  5.2 0.0 copy-done.2
  5.2 1.0 copy_bitcast_fusion.2
  6.2 0.0 copy-done.3
  6.2 0.0 copy-done.4
  6.2 1.0 copy_bitcast_fusion
  7.2 220.8 %shard_map.127 = bf16[192,2048]{1,0:T(8,128)(2,1)} custom-call(f32[2,2]{1,0:T(2,128)} %lam_ref.1, f32[2,2,128]{2,1,0:T(2,128)} %gain_ref.1, f32[2,2048]{1,0:T(2,128)} %norm_ref.1, bf16[192,2048]{1,0:T(8,128)(2,1)} %residual_in.1, bf16[2,768,128]{2,1,0:T(8,128)(2,1)} %get-tuple-element.8.qf, bf16[2,768,128]{2,1,0:T(8,128)(2,1)} %get-tuple-element.7.kf, ...), custom_call_target="tpu_custom_call" | custom-call | tf_op jit(solution)/shard_map/pallas_call | solution.py:716
  228.1 2.1 copy.31
Async XLA Ops:
  0.0 3.5 %copy-start = (bf16[768,2,256]{2,1,0:T(2,128)(2,1)S(1)}, bf16[768,2,256]{2,1,0:T(2,128)(2,1)}, u32[]{:S(2)}) copy-start(bf16[768,2,256]{2,1,0:T(2,128)(2,1)} %param.17) | copy-start | bytes 2359300
  2.3 2.9 %copy-start.1 = (bf16[768,2,128]{2,1,0:T(2,128)(2,1)S(1)}, bf16[768,2,128]{2,1,0:T(2,128)(2,1)}, u32[]{:S(2)}) copy-start(bf16[768,2,128]{2,1,0:T(2,128)(2,1)} %param.14) | copy-start | bytes 1179652
  2.3 2.9 %copy-start.2 = (bf16[768,2,128]{2,1,0:T(2,128)(2,1)S(1)}, bf16[768,2,128]{2,1,0:T(2,128)(2,1)}, u32[]{:S(2)}) copy-start(bf16[768,2,128]{2,1,0:T(2,128)(2,1)} %param.13) | copy-start | bytes 1179652
  3.5 2.8 %copy-start.3 = (bf16[768,2,128]{2,1,0:T(2,128)(2,1)S(1)}, bf16[768,2,128]{2,1,0:T(2,128)(2,1)}, u32[]{:S(2)}) copy-start(bf16[768,2,128]{2,1,0:T(2,128)(2,1)} %param.18) | copy-start | bytes 1179652
  3.5 2.8 %copy-start.4 = (bf16[768,2,128]{2,1,0:T(2,128)(2,1)S(1)}, bf16[768,2,128]{2,1,0:T(2,128)(2,1)}, u32[]{:S(2)}) copy-start(bf16[768,2,128]{2,1,0:T(2,128)(2,1)} %param.15) | copy-start | bytes 1179652
